TPU v7x, 128 devices: a whole 4x4x4 slice. The times are simulated.
128 devices in a mesh: sp: 64 (over z, y, x), tp: 2 (over core).
Axes of the slice: x: 4, y: 4, z: 4, core: 2. Of those that a mesh axis runs over, the one named last changes fastest.
Arguments:
- residual: bfloat16 [16384, 2048], P(('sp', 'tp')), may hold values from -6 to 6
- queries: bfloat16 [16384, 1152], P('sp', 'tp'), may hold values from -800 to 800
- latent: bfloat16 [16384, 256], P('sp'), may hold values from -6 to 6
- rope_key: bfloat16 [16384, 32], P('sp'), may hold values from -6 to 6
- doc_ids: int32 [16384], P('sp'), may hold values from 0 to 5, never falling along the last dimension, each value on 1 to 8192 neighbouring positions
- latent_to_key: bfloat16 [256, 768], P(None, 'tp'), may hold values from -0.375 to 0.375
- latent_to_value: bfloat16 [256, 768], P(None, 'tp'), may hold values from -0.375 to 0.375
- out_proj: bfloat16 [768, 2048], replicated, may hold values from -0.21875 to 0.21875
- mix_gain: float32 [2048], replicated, may hold values from 0.1 to 1.9
- moe_gain: float32 [2048], replicated, may hold values from 0.1 to 1.9
- expert_ids: int32 [16384, 2], P(('sp', 'tp')), may hold values from 0 to 63, as said below
- route_weight: float32 [16384, 2], P(('sp', 'tp')), may hold values from 0.1 to 1
- gate_weight: bfloat16 [64, 2048, 1024], P('sp', None, 'tp'), may hold values from -0.125 to 0.125
- up_weight: bfloat16 [64, 2048, 1024], P('sp', None, 'tp'), may hold values from -0.125 to 0.125
- down_weight: bfloat16 [64, 1024, 2048], P('sp', 'tp'), may hold values from -0.1875 to 0.1875
Outputs:
- output: bfloat16 [16384, 2048], P(('sp', 'tp'))
Inputs may be any that keep to these rules, and one draw needn't show every extreme that they name: `expert_ids`: each row names 2 different experts of one group of 16 consecutive numbers; in each aligned block of 128 rows (the rows of one device) no expert is named more than 8 times, and some expert exactly 8 times.
All inputs are finite; a program needn't handle non-finite values.
Results may differ from a plain program's by a relative error of at most 0.013.
Values may be sent and summed in bfloat16 or wider, within the bound.
A program may use at most 64 MiB of HBM per device.

v0:
```python
import math
import jax
import jax.numpy as jnp
from jax import lax
from jax.sharding import PartitionSpec as P

D = 2048
UNROTATED_DIM = 64
ROPE = 32
VALUE_ENTRIES = 64
GROUPS = 4
rope_base = 10000.0
epsilon = 1e-06


def in_order(pieces, dim):
    pieces = jnp.moveaxis(pieces, 0, dim)
    lengths = pieces.shape
    return pieces.reshape(*lengths[:dim], lengths[dim] * lengths[dim + 1], *lengths[dim + 2 :])


def sent_to_all(x, axis):
    size = lax.axis_size(axis)
    return lax.all_to_all(jnp.broadcast_to(x[None], (size, *x.shape)), axis, 0, 0, tiled=True)


def collect(x, axis, dim):
    return in_order(sent_to_all(x, axis), dim)


def cut_along(x, dim, size):
    before, after = (x.shape[:dim], x.shape[dim + 1 :])
    return jnp.moveaxis(x.reshape(*before, size, -1, *after), dim, 0)


def sum_at_owner(x, axis, dim):
    pieces = cut_along(x, dim, lax.axis_size(axis))
    arrived = lax.all_to_all(pieces, axis, split_axis=0, concat_axis=0, tiled=True)
    return arrived.astype(jnp.float32).sum(axis=0)


def rotate(source, positions):
    half_width = source.shape[-1] // 2
    frequency = rope_base ** (-jnp.arange(half_width, dtype=jnp.float32) / half_width)
    angles = positions.astype(jnp.float32)[:, None] * frequency[None, :]
    if source.ndim == 3:
        angles = angles[:, None, :]
    cosine = jnp.cos(angles)
    sine_part = jnp.sin(angles)
    upper_half = source[..., :half_width].astype(jnp.float32)
    lower_half = source[..., half_width:].astype(jnp.float32)
    turned = jnp.concatenate(
        [
            upper_half * cosine - lower_half * sine_part,
            lower_half * cosine + upper_half * sine_part,
        ],
        axis=-1,
    )
    return turned.astype(jnp.bfloat16)


def rms_scale(source, gain):
    return source * lax.rsqrt(jnp.mean(source * source, axis=-1, keepdims=True) + epsilon) * gain


def attend_keys(
    running,
    query_nope,
    query_rot,
    query_pos,
    query_docs,
    key_nope,
    key_rot,
    value_rows,
    key_pos,
    key_docs,
):
    row_max, row_total, weighted = running
    score_scale = (UNROTATED_DIM + ROPE) ** (-0.5)
    scores = (
        jnp.einsum("qhd,khd->qhk", query_nope, key_nope, preferred_element_type=jnp.float32)
        + jnp.einsum("qhr,kr->qhk", query_rot, key_rot, preferred_element_type=jnp.float32)
    ) * score_scale
    allowed = (
        (key_pos[None, :] <= query_pos[:, None]) & (key_docs[None, :] == query_docs[:, None])
    )[:, None, :]
    new_max = jnp.maximum(row_max, jnp.max(jnp.where(allowed, scores, -1e30), axis=-1))
    weights = jnp.where(allowed, jnp.exp(scores - new_max[..., None]), 0.0)
    factor = jnp.exp(row_max - new_max)
    row_total = row_total * factor + jnp.sum(weights, axis=-1)
    weighted = weighted * factor[..., None] + jnp.einsum(
        "qhk,khd->qhd", weights.astype(jnp.bfloat16), value_rows, preferred_element_type=jnp.float32
    )
    return (new_max, row_total, weighted)


def local(
    residual,
    queries,
    latent,
    rope_key,
    doc_ids,
    latent_to_key,
    latent_to_value,
    out_proj,
    mix_gain,
    moe_gain,
    expert_ids,
    route_weight,
    gate_weight,
    up_weight,
    down_weight,
):
    local_rows = queries.shape[0]
    local_heads = queries.shape[1] // (UNROTATED_DIM + ROPE)
    query_pos = lax.axis_index("sp") * local_rows + jnp.arange(local_rows, dtype=jnp.int32)
    shaped = queries.reshape(local_rows, local_heads, UNROTATED_DIM + ROPE)
    query_nope = shaped[..., :UNROTATED_DIM]
    query_rot = rotate(shaped[..., UNROTATED_DIM:], query_pos)
    key_rot = rotate(rope_key, query_pos)
    initial = (
        jnp.full((local_rows, local_heads), -1e30, jnp.float32),
        jnp.zeros((local_rows, local_heads), jnp.float32),
        jnp.zeros((local_rows, local_heads, VALUE_ENTRIES), jnp.float32),
    )
    pieces = (
        lax.all_gather(latent, "sp", axis=0, tiled=True),
        lax.all_gather(key_rot, "sp", axis=0, tiled=True),
        lax.all_gather(doc_ids, "sp", axis=0, tiled=True),
    )
    row_count = pieces[0].shape[0]
    block_rows = math.gcd(row_count, 512)

    def one_block(number, current):
        first_row = number * block_rows
        sliced = [lax.dynamic_slice_in_dim(member, first_row, block_rows, 0) for member in pieces]
        key_pos = first_row + jnp.arange(block_rows, dtype=jnp.int32)
        active = (first_row <= query_pos[-1]) & (sliced[-1][-1] >= doc_ids[0])

        def compute(carried):
            key_nope = jnp.dot(sliced[0], latent_to_key, preferred_element_type=jnp.float32).astype(
                jnp.bfloat16
            )
            value_rows = jnp.dot(
                sliced[0], latent_to_value, preferred_element_type=jnp.float32
            ).astype(jnp.bfloat16)
            key_part = sliced[1]
            return attend_keys(
                carried,
                query_nope,
                query_rot,
                query_pos,
                doc_ids,
                key_nope.reshape(block_rows, local_heads, UNROTATED_DIM),
                key_part,
                value_rows.reshape(block_rows, local_heads, VALUE_ENTRIES),
                key_pos,
                sliced[-1],
            )

        return lax.cond(active, compute, lambda carried: carried, current)

    running = lax.fori_loop(0, row_count // block_rows, one_block, initial)
    attended = (running[2] / running[1][..., None]).astype(jnp.bfloat16)
    attended = attended.reshape(local_rows, local_heads * VALUE_ENTRIES)
    gathered = lax.all_to_all(attended, "tp", split_axis=0, concat_axis=1, tiled=True)
    mix = jnp.dot(gathered, out_proj, preferred_element_type=jnp.float32)
    branch = rms_scale(mix, mix_gain)
    middle = lax.optimization_barrier((residual.astype(jnp.float32) + branch).astype(jnp.bfloat16))
    normed = rms_scale(middle.astype(jnp.float32), moe_gain).astype(jnp.bfloat16)
    row_count = normed.shape[0]
    top_count = expert_ids.shape[1]
    expert_count = lax.axis_size("sp")
    capacity = row_count // (expert_count // GROUPS)
    flat_ids = expert_ids.reshape(-1)
    onehot = (flat_ids[:, None] == jnp.arange(expert_count, dtype=jnp.int32)[None, :]).astype(
        jnp.int32
    )
    earlier = jnp.cumsum(onehot, axis=0) - onehot
    slot_rank = jnp.sum(earlier * onehot, axis=1)
    slot_ids = (flat_ids * capacity + slot_rank).reshape(row_count, top_count)
    chooser = jnp.any(
        jnp.arange(expert_count * capacity, dtype=jnp.int32)[:, None, None] == slot_ids[None],
        axis=2,
    ).astype(jnp.bfloat16)
    buffer = jnp.dot(chooser, normed, preferred_element_type=jnp.float32).astype(jnp.bfloat16)
    buffer = buffer.reshape(expert_count, capacity, D)
    arrived = lax.all_to_all(buffer, "sp", split_axis=0, concat_axis=0, tiled=True)
    model_width = arrived.shape[2]
    both_halves = collect(arrived, "tp", 0)
    flat_rows = both_halves.reshape(-1, model_width)
    gate_out = jnp.dot(flat_rows, gate_weight[0], preferred_element_type=jnp.float32)
    upward = jnp.dot(flat_rows, up_weight[0], preferred_element_type=jnp.float32)
    hidden = (jax.nn.silu(gate_out) * upward).astype(jnp.bfloat16)
    partial_value = jnp.dot(hidden, down_weight[0], preferred_element_type=jnp.float32).reshape(
        both_halves.shape
    )
    summed = sum_at_owner(partial_value.astype(jnp.bfloat16), "tp", 0).astype(jnp.bfloat16)
    returned = lax.all_to_all(summed, "sp", split_axis=0, concat_axis=0, tiled=True)
    picked = returned.reshape(-1, D)[slot_ids.reshape(-1)].astype(jnp.float32)
    expert_mix = jnp.sum(
        (picked * route_weight.reshape(-1)[:, None]).reshape(row_count, top_count, D), axis=1
    )
    return (middle.astype(jnp.float32) + expert_mix).astype(jnp.bfloat16)


def solution(mesh):
    in_specs = (
        P(("sp", "tp"), None),
        P("sp", "tp"),
        P("sp", None),
        P("sp", None),
        P("sp"),
        P(None, "tp"),
        P(None, "tp"),
        P(),
        P(),
        P(),
        P(("sp", "tp"), None),
        P(("sp", "tp"), None),
        P("sp", None, "tp"),
        P("sp", None, "tp"),
        P("sp", "tp", None),
    )
    out_specs = P(("sp", "tp"), None)
    return jax.shard_map(local, mesh=mesh, in_specs=in_specs, out_specs=out_specs, check_vma=False)
```

profile of v0, /device:TPU:0, one launch (start us, length us, event | category | flops | bytes accessed | tf_op | source)
XLA Modules:
  0.0 649.7 jit_solution(9027320513454528965)
XLA Ops:
  10.0 1.6 slice.54
  13.5 186.6 %all-gather = s32[64,1,256]{2,1,0:T(1,128)} all-gather(s32[1,1,256]{2,1,0:T(1,128)} %bitcast.92), channel_id=1, replica_groups=mesh['sp'=64,'tp'=2] {'sp'}, dimensions={0}, use_global_device_ids=true | all-gather | bytes 66560 | tf_op jit(solution)/shard_map/all_gather | solution.py:129
  202.9 216.7 %while.17 = (s32[]{:T(128)}, f32[256,6]{0,1:T(8,128)S(1)}, f32[256,6]{0,1:T(8,128)S(1)}, f32[256,6,64]{0,2,1:T(8,128)S(1)}, s32[256]{0:T(256)}, /*index=5*/s32[1...) while((s32[]{:T(128)}, f32[256,6]{0,1:T(8,128)S(1)}, ...), condition=%wide.region_5.6_spmd, body=%wide.region_0.5_spmd.sunk | while | flops 461835776 | bytes 21579896 | solution.py:163
  207.4 1.3 slice.70
  209.5 7.0 %conditional.2 = ((f32[256,6]{0,1:T(8,128)S(1)}, f32[256,6]{0,1:T(8,128)S(1)}, f32[256,6,64]{0,2,1:T(8,128)S(1)})) conditional(s32[]{:T(128)} %convert_element_type.177, (f32[256,6]{0,1:T(8,128)S(1)}, f32[256,6]{0,1:T(8,128)S(1)}, f32[256,6,64]{0,2,1:T(8,128)S(1)}) %tuple.50, (s32[]{:T(128)}, s32[512]{0:T(512)}, s32[256]{0:T(256)}, s32[512]{0:T(512)}, ...), branch_computations={%region_1.0_spmd, %region_2.4_spmd} | conditional | flops 461835776 | bytes 21565132 | solution.py:161
  209.5 1.3 convolution_convert_fusion.1
  210.9 1.5 fusion.16
  221.0 1.3 slice.70
  227.5 1.3 slice.70
  234.1 1.3 slice.70
  240.6 1.3 slice.70
  247.2 1.3 slice.70
  253.7 1.3 slice.70
  260.3 1.3 slice.70
  266.8 1.3 slice.70
  273.4 1.3 slice.70
  279.9 1.3 slice.70
  286.5 1.3 slice.70
  421.4 4.0 all_to_all.39
  428.0 137.1 %all_to_all.40 = bf16[64,8,2048]{2,1,0:T(8,128)(2,1)S(1)} all-to-all(bf16[64,8,2048]{2,1,0:T(8,128)(2,1)S(1)} %fusion.23), channel_id=1, replica_groups=mesh['sp'=64,'tp'=2] {'sp'}, dimensions={0} | all-to-all | bytes 4194304 | tf_op jit(solution)/shard_map/all_to_all | solution.py:188
  565.6 7.2 %all_to_all.41 = bf16[2,64,8,2048]{3,2,1,0:T(8,128)(2,1)S(1)} all-to-all(bf16[2,64,8,2048]{3,2,1,0:T(8,128)(2,1)S(1)} %broadcast_in_dim.63), channel_id=1, replica_groups=mesh['sp'=64,'tp'=2] {'tp'}, dimensions={0} | all-to-all | bytes 8388608 | tf_op jit(solution)/shard_map/all_to_all | solution.py:24
  572.8 2.3 fusion.25
  575.2 2.6 fusion.31
  577.8 2.4 convolution_convert_fusion.2
  580.8 8.2 %all_to_all.42 = bf16[2,64,8,2048]{3,1,2,0:T(8,128)(2,1)} all-to-all(bf16[2,64,8,2048]{3,1,2,0:T(8,128)(2,1)S(1)} %copy.65), channel_id=1, replica_groups=mesh['sp'=64,'tp'=2] {'tp'}, dimensions={0} | all-to-all | bytes 8388608 | tf_op jit(solution)/shard_map/all_to_all | solution.py:38
  589.0 3.5 reduce_sum.67
  592.5 2.5 copy.67
  595.0 6.1 all-to-all-start.4
  601.3 29.9 %all-to-all-done.4 = bf16[64,8,2048]{2,1,0:T(8,128)(2,1)S(1)} async-done(((bf16[64,8,2048]{2,1,0:T(8,128)(2,1)}), bf16[64,8,2048]{2,1,0:T(8,128)(2,1)S(1)}, u32[]{:S(2)}, u32[]{:S(2)}) %all-to-all-start.4) | async-done | bytes 2097184 | tf_op jit(solution)/shard_map/all_to_all | solution.py:199
  631.2 2.3 gather_fusion
  633.5 3.5 reshape.226
  637.1 4.9 multiply_reduce_fusion
  (339 shorter events, 148.3 us)
Async XLA Ops:
  6.5 418.9 %copy-start = (bf16[768,2048]{1,0:T(8,128)(2,1)S(1)}, bf16[768,2048]{1,0:T(8,128)(2,1)}, u32[]{:S(2)}) copy-start(bf16[768,2048]{1,0:T(8,128)(2,1)} %param.26) | copy-start | bytes 9437188
  6.5 196.3 %all-gather.6.cloned.1.call-start = ((), (), s32[]{:S(2)}) async-start(), calls=%async_computation.6 | async-start | bytes 1064960 | tf_op jit(solution)/shard_map/all_gather | solution.py:128
  8.2 194.6 %all-gather.4.cloned.1.call-start = ((), (), s32[]{:S(2)}) async-start(), calls=%async_computation.5 | async-start | bytes 8519680 | tf_op jit(solution)/shard_map/all_gather | solution.py:127
  12.6 190.2 %copy-start.14 = (s32[256]{0:T(256)}, s32[256]{0:T(256)S(1)}, u32[]{:S(2)}) copy-start(s32[256]{0:T(256)S(1)} %fusion.49) | copy-start | bytes 3076
  203.7 0.6 copy-start.9
  209.5 2.9 copy-start.11
  209.5 2.9 copy-start.10
  209.5 2.9 copy-start.12
  209.5 2.9 copy-start.13
  209.5 3.1 copy-start.4
  213.5 0.9 copy-start.5
  289.3 0.6 copy-start.9
  328.7 0.6 copy-start.9
  348.4 0.6 copy-start.9
  354.9 0.6 copy-start.9
  361.5 0.6 copy-start.9
  368.0 0.6 copy-start.9
  394.2 0.6 copy-start.9
  419.7 6.5 copy-start.16
  421.4 4.8 copy-start.6
  425.5 1.7 copy-start.7
  425.5 1.7 copy-start.17
  426.4 0.8 copy-start.2
  565.6 7.2 %copy-start.19 = (bf16[1,2048,512]{2,1,0:T(8,128)(2,1)S(1)}, bf16[1,2048,512]{2,1,0:T(8,128)(2,1)}, u32[]{:S(2)}) copy-start(bf16[1,2048,512]{2,1,0:T(8,128)(2,1)} %param.32) | copy-start | bytes 6291460
  572.8 2.3 copy-start.20
  575.2 2.7 copy-start.21
  595.0 6.1 copy-start.8
  595.0 6.2 copy-start.18
  595.0 6.4 copy-start.15
  595.0 36.2 %all-to-all-start.4 = ((bf16[64,8,2048]{2,1,0:T(8,128)(2,1)}), bf16[64,8,2048]{2,1,0:T(8,128)(2,1)S(1)}, u32[]{:S(2)}, u32[]{:S(2)}) async-start(bf16[64,8,2048]{2,1,0:T(8,128)(2,1)} %copy.67), calls=%async_computation.4 | async-start | bytes 4194304 | tf_op jit(solution)/shard_map/all_to_all | solution.py:199
  633.5 9.3 %copy-start.1 = (bf16[768,2048]{1,0:T(8,128)(2,1)S(1)}, bf16[768,2048]{1,0:T(8,128)(2,1)}, u32[]{:S(2)}) copy-start(bf16[768,2048]{1,0:T(8,128)(2,1)} %param.26) | copy-start | bytes 9437188
  637.1 4.9 copy-start.3
  (24 other events, 14.4 us)
Sparse Core Ops, SparseCore 0:
  10.0 66.1 all-gather.5
  79.0 76.5 all-gather.3
where the time goes:
time: 655 us; the launch traced here: 650 us
  blocking collectives  343 us (52%)
  local copies, waits for them, and re-layouts  160 us (24%)
  loops' own time  64.4 us (10%)
  waiting for transfers between devices  30.6 us (5%)
  other arithmetic  17 us (3%)
  matrix products  14.5 us (2%)
  between operations  13.7 us (2%)
    all_gather x1, blocking collectives, local(): lax.all_gather(doc_ids, 'sp', axis=0, tiled=True)  187 us
    all_to_all x1, blocking collectives, local(): lax.all_to_all(buffer, 'sp', split_axis=0, concat_axis=0, tiled=True)  137 us
    slice x96, local copies, waits for them, and re-layouts, one_block(): active = (first_row <= query_pos[-1]) & (sliced[-1][-1] >= doc_ids[0])  102 us
    another operation x1, loops' own time, local(): running = lax.fori_loop(0, row_count // block_rows, one_block, initial)  63.9 us
    all_to_all x1, waiting for transfers between devices, local(): lax.all_to_all(summed, 'sp', split_axis=0, concat_axis=0, tiled=True)  29.9 us
    dynamic_slice x32, local copies, waits for them, and re-layouts, one_block(): lax.dynamic_slice_in_dim(member, first_row, block_rows, 0)  24.2 us
    iota x32, local copies, waits for them, and re-layouts, one_block(): key_pos = first_row + jnp.arange(block_rows, dtype=jnp.int32)  19.1 us
  transfers between devices with their start and end apart: 3, of which 1 were waited for; matrix products, arithmetic and copies ran while one was open for 1% of the time, Pallas kernels for 0%

commit v1 on v0

--- a/solution.py
+++ b/solution.py
@@ -1,3 +1,4 @@
+import functools
 import math
 import jax
 import jax.numpy as jnp
@@ -11,6 +12,26 @@
 GROUPS = 4
 rope_base = 10000.0
 epsilon = 1e-06
+
+
+def group_the_pages(message, axis_key, where_dim):
+    aux, reached = (lax.axis_size(axis_key), lax.axis_index(axis_key))
+    new, response = (message, 1)
+    while response < aux:
+        items = []
+        i = 0
+        while i < aux:
+            items.append((i, i ^ response))
+            i = i + 1
+        wide_out = lax.ppermute(new, axis_key, items)
+        v_now = jnp.concatenate([new, wide_out], axis=where_dim)
+        r1 = jnp.concatenate([wide_out, new], where_dim)
+        new = jnp.where(reached & response == 0, v_now, r1)
+        response = 2 * response
+    return new
+
+
+remake_patch = functools.partial(group_the_pages, axis_key="sp", where_dim=0)
 
 
 def in_order(pieces, dim):
@@ -126,7 +147,7 @@
     pieces = (
         lax.all_gather(latent, "sp", axis=0, tiled=True),
         lax.all_gather(key_rot, "sp", axis=0, tiled=True),
-        lax.all_gather(doc_ids, "sp", axis=0, tiled=True),
+        remake_patch(doc_ids),
     )
     row_count = pieces[0].shape[0]
     block_rows = math.gcd(row_count, 512)

time: 655 us -> 598 us (0.913)
  blocking collectives: 343 us -> 163 us
  waiting for transfers between devices: 30.6 us -> 153 us
  starting transfers between devices: 6.11 us -> 21.8 us
  local copies, waits for them, and re-layouts: 160 us -> 152 us
  loops' own time: 64.4 us -> 56.9 us
    all_gather x1 -> x0, blocking collectives: 187 us -> none  [local(): lax.all_gather(doc_ids, 'sp', axis=0, tiled=True)]
    all_gather x1, waiting for transfers between devices: 0.01 us -> 79.3 us  [local(): lax.all_gather(latent, 'sp', axis=0, tiled=True)]
    all_gather x1, waiting for transfers between devices: 0.01 us -> 38.2 us  [local(): lax.all_gather(key_rot, 'sp', axis=0, tiled=True)]
    ppermute x0 -> x6, starting transfers between devices: none -> 15.7 us  [group_the_pages(): wide_out = lax.ppermute(new, axis_key, items)]
    slice x96, local copies, waits for them, and re-layouts: 102 us -> 94.5 us  [one_block(): active = (first_row <= query_pos[-1]) & (sliced[-1][-1] >= doc_ids[0])]
    another operation x1, loops' own time: 63.9 us -> 56.4 us  [local(): running = lax.fori_loop(0, row_count // block_rows, one_block, initial)]
  transfers between devices with their start and end apart: 3 -> 9, of which waited for: 1 -> 7; matrix products, arithmetic and copies ran while one was open for 1% -> 1% of each run, Pallas kernels for 0% -> 0%
where the time goes in v1:
time: 598 us; the launch traced here: 593 us
  blocking collectives  163 us (27%)
  waiting for transfers between devices  153 us (26%)
  local copies, waits for them, and re-layouts  152 us (25%)
  loops' own time  56.9 us (10%)
  starting transfers between devices  21.8 us (4%)
  other arithmetic  18.3 us (3%)
  matrix products  14.5 us (2%)
  between operations  13.7 us (2%)
    all_to_all x1, blocking collectives, local(): lax.all_to_all(buffer, 'sp', split_axis=0, concat_axis=0, tiled=True)  143 us
    slice x96, local copies, waits for them, and re-layouts, one_block(): active = (first_row <= query_pos[-1]) & (sliced[-1][-1] >= doc_ids[0])  94.5 us
    all_gather x1, waiting for transfers between devices, local(): lax.all_gather(latent, 'sp', axis=0, tiled=True)  79.3 us
    another operation x1, loops' own time, local(): running = lax.fori_loop(0, row_count // block_rows, one_block, initial)  56.4 us
    all_gather x1, waiting for transfers between devices, local(): lax.all_gather(key_rot, 'sp', axis=0, tiled=True)  38.2 us
    all_to_all x1, waiting for transfers between devices, local(): lax.all_to_all(summed, 'sp', split_axis=0, concat_axis=0, tiled=True)  29.9 us
    dynamic_slice x32, local copies, waits for them, and re-layouts, one_block(): lax.dynamic_slice_in_dim(member, first_row, block_rows, 0)  24.2 us
    iota x32, local copies, waits for them, and re-layouts, one_block(): key_pos = first_row + jnp.arange(block_rows, dtype=jnp.int32)  16.7 us
  transfers between devices with their start and end apart: 9, of which 7 were waited for; matrix products, arithmetic and copies ran while one was open for 1% of the time, Pallas kernels for 0%

profile of v1, /device:TPU:0, one launch (start us, length us, event | category | flops | bytes accessed | tf_op | source)
XLA Modules:
  0.0 592.8 jit_solution(16967365003415645047)
XLA Ops:
  9.0 1.7 collective-permute-start
  13.6 3.1 collective-permute-start.1
  17.3 1.4 collective-permute-done.1
  18.7 1.7 collective-permute-start.2
  22.3 3.3 collective-permute-start.3
  27.5 2.0 collective-permute-start.4
  31.2 4.0 collective-permute-start.5
  35.8 1.6 slice.54
  38.0 38.2 %all-gather.5.cloned.1.call-done = bf16[16384,32]{0,1:T(8,128)(2,1)} async-done(((bf16[256,32]{0,1:T(8,128)(2,1)}), bf16[16384,32]{0,1:T(8,128)(2,1)}) %all-gather.5.cloned.1.call-update) | async-done | bytes 1048592 | tf_op jit(solution)/shard_map/all_gather | solution.py:149
  76.2 79.3 %all-gather.3.cloned.1.call-done = bf16[16384,256]{1,0:T(8,128)(2,1)} async-done(((bf16[256,256]{1,0:T(8,128)(2,1)}), bf16[16384,256]{1,0:T(8,128)(2,1)}) %all-gather.3.cloned.1.call-update) | async-done | bytes 8388624 | tf_op jit(solution)/shard_map/all_gather | solution.py:148
  155.6 201.2 %while.17 = (s32[]{:T(128)}, f32[256,6]{0,1:T(8,128)S(1)}, f32[256,6]{0,1:T(8,128)S(1)}, f32[256,6,64]{0,2,1:T(8,128)S(1)}, s32[256]{0:T(256)}, /*index=5*/s32[1...) while((s32[]{:T(128)}, f32[256,6]{0,1:T(8,128)S(1)}, ...), condition=%wide.region_5.6_spmd, body=%wide.region_0.5_spmd.sunk | while | flops 461835776 | bytes 21579896 | solution.py:184
  161.6 7.0 %conditional.2 = ((f32[256,6]{0,1:T(8,128)S(1)}, f32[256,6]{0,1:T(8,128)S(1)}, f32[256,6,64]{0,2,1:T(8,128)S(1)})) conditional(s32[]{:T(128)} %convert_element_type.177, (f32[256,6]{0,1:T(8,128)S(1)}, f32[256,6]{0,1:T(8,128)S(1)}, f32[256,6,64]{0,2,1:T(8,128)S(1)}) %tuple.50, (s32[]{:T(128)}, s32[512]{0:T(512)}, s32[256]{0:T(256)}, s32[512]{0:T(512)}, ...), branch_computations={%region_1.1_spmd, %region_2.4_spmd} | conditional | flops 461835776 | bytes 21565132 | solution.py:182
  161.7 1.3 convolution_convert_fusion.1
  163.0 1.5 fusion.16
  166.6 1.2 convolution_convert_fusion
  172.9 1.2 slice.70
  179.0 1.2 slice.70
  185.1 1.2 slice.70
  358.6 4.0 all_to_all.39
  365.1 143.1 %all_to_all.40 = bf16[64,8,2048]{2,1,0:T(8,128)(2,1)S(1)} all-to-all(bf16[64,8,2048]{2,1,0:T(8,128)(2,1)S(1)} %fusion.23), channel_id=1, replica_groups=mesh['sp'=64,'tp'=2] {'sp'}, dimensions={0} | all-to-all | bytes 4194304 | tf_op jit(solution)/shard_map/all_to_all | solution.py:209
  508.8 7.2 %all_to_all.41 = bf16[2,64,8,2048]{3,2,1,0:T(8,128)(2,1)S(1)} all-to-all(bf16[2,64,8,2048]{3,2,1,0:T(8,128)(2,1)S(1)} %broadcast_in_dim.63), channel_id=1, replica_groups=mesh['sp'=64,'tp'=2] {'tp'}, dimensions={0} | all-to-all | bytes 8388608 | tf_op jit(solution)/shard_map/all_to_all | solution.py:45
  516.0 2.3 fusion.25
  518.4 2.6 fusion.31
  521.1 2.4 convolution_convert_fusion.2
  524.0 8.1 %all_to_all.42 = bf16[2,64,8,2048]{3,1,2,0:T(8,128)(2,1)} all-to-all(bf16[2,64,8,2048]{3,1,2,0:T(8,128)(2,1)S(1)} %copy.65), channel_id=1, replica_groups=mesh['sp'=64,'tp'=2] {'tp'}, dimensions={0} | all-to-all | bytes 8388608 | tf_op jit(solution)/shard_map/all_to_all | solution.py:59
  532.2 3.5 reduce_sum.67
  535.6 2.5 copy.67
  538.1 6.1 %all-to-all-start.4 = ((bf16[64,8,2048]{2,1,0:T(8,128)(2,1)}), bf16[64,8,2048]{2,1,0:T(8,128)(2,1)S(1)}, u32[]{:S(2)}, u32[]{:S(2)}) async-start(bf16[64,8,2048]{2,1,0:T(8,128)(2,1)} %copy.67), calls=%async_computation.4 | async-start | bytes 4194304 | tf_op jit(solution)/shard_map/all_to_all | solution.py:220
  544.5 29.9 %all-to-all-done.4 = bf16[64,8,2048]{2,1,0:T(8,128)(2,1)S(1)} async-done(((bf16[64,8,2048]{2,1,0:T(8,128)(2,1)}), bf16[64,8,2048]{2,1,0:T(8,128)(2,1)S(1)}, u32[]{:S(2)}, u32[]{:S(2)}) %all-to-all-start.4) | async-done | bytes 2097184 | tf_op jit(solution)/shard_map/all_to_all | solution.py:220
  574.4 2.3 gather_fusion
  576.7 3.5 reshape.226
  580.2 4.9 multiply_reduce_fusion
  (356 shorter events, 156.2 us)
Async XLA Ops:
  6.5 356.1 %copy-start = (bf16[768,2048]{1,0:T(8,128)(2,1)S(1)}, bf16[768,2048]{1,0:T(8,128)(2,1)}, u32[]{:S(2)}) copy-start(bf16[768,2048]{1,0:T(8,128)(2,1)} %param.26) | copy-start | bytes 9437188
  6.5 69.6 %all-gather.5.cloned.1.call-start = ((), (), s32[]{:S(2)}) async-start(), calls=%async_computation.6 | async-start | bytes 1064960 | tf_op jit(solution)/shard_map/all_gather | solution.py:149
  8.2 147.3 %all-gather.3.cloned.1.call-start = ((), (), s32[]{:S(2)}) async-start(), calls=%async_computation.5 | async-start | bytes 8519680 | tf_op jit(solution)/shard_map/all_gather | solution.py:148
  9.0 3.9 collective-permute-start
  12.7 63.5 %copy-start.14 = (s32[256]{0:T(256)}, s32[256]{0:T(256)S(1)}, u32[]{:S(2)}) copy-start(s32[256]{0:T(256)S(1)} %fusion.49) | copy-start | bytes 3076
  13.6 5.1 collective-permute-start.1
  18.7 3.6 collective-permute-start.2
  22.3 5.2 collective-permute-start.3
  27.5 3.7 collective-permute-start.4
  31.2 6.2 %collective-permute-start.5 = (s32[8192]{0:T(1024)S(1)}, s32[8192]{0:T(1024)S(1)}, u32[]{:S(2)}, u32[]{:S(2)}) collective-permute-start(s32[8192]{0:T(1024)S(1)} %add_select_fusion.1), channel_id=1, source_target_pairs={{0,64},{2,66},{4,68},{6,70},{8,72},{10,74},{12,76},{14,78},{16,80}... | collective-permute-start | bytes 98312 | tf_op jit(solution)/shard_map/ppermute | solution.py:26
  156.3 0.6 copy-start.9
  161.6 2.9 copy-start.11
  161.6 2.9 copy-start.10
  161.6 2.9 copy-start.12
  161.7 2.9 copy-start.13
  161.7 3.1 copy-start.4
  165.7 0.9 copy-start.5
  169.4 0.6 copy-start.9
  356.8 6.5 %copy-start.16 = (f32[2048]{0:T(1024)S(1)}, f32[2048]{0:T(1024)}, u32[]{:S(2)}) copy-start(f32[2048]{0:T(1024)} %param.27) | copy-start | bytes 24580
  358.5 4.8 copy-start.6
  362.6 1.7 copy-start.7
  362.6 1.7 copy-start.17
  363.5 0.8 copy-start.2
  508.8 7.2 %copy-start.19 = (bf16[1,2048,512]{2,1,0:T(8,128)(2,1)S(1)}, bf16[1,2048,512]{2,1,0:T(8,128)(2,1)}, u32[]{:S(2)}) copy-start(bf16[1,2048,512]{2,1,0:T(8,128)(2,1)} %param.32) | copy-start | bytes 6291460
  516.0 2.3 copy-start.20
  518.4 2.7 copy-start.21
  538.1 6.1 %copy-start.8 = (s32[128,2]{1,0:T(8,128)S(1)}, s32[128,2]{1,0:T(8,128)}, u32[]{:S(2)}) copy-start(s32[128,2]{1,0:T(8,128)} %get-tuple-element.385) | copy-start | bytes 3076
  538.1 6.2 %copy-start.18 = (f32[128,2]{0,1:T(2,128)S(1)}, f32[128,2]{0,1:T(2,128)}, u32[]{:S(2)}) copy-start(f32[128,2]{0,1:T(2,128)} %param.30) | copy-start | bytes 3076
  538.1 6.4 %copy-start.15 = (s32[256]{0:T(256)S(1)}, s32[256]{0:T(256)}, u32[]{:S(2)}) copy-start(s32[256]{0:T(256)} %copy-done.14) | copy-start | bytes 3076
  538.1 36.2 %all-to-all-start.4 = ((bf16[64,8,2048]{2,1,0:T(8,128)(2,1)}), bf16[64,8,2048]{2,1,0:T(8,128)(2,1)S(1)}, u32[]{:S(2)}, u32[]{:S(2)}) async-start(bf16[64,8,2048]{2,1,0:T(8,128)(2,1)} %copy.67), calls=%async_computation.4 | async-start | bytes 4194304 | tf_op jit(solution)/shard_map/all_to_all | solution.py:220
  576.7 9.3 %copy-start.1 = (bf16[768,2048]{1,0:T(8,128)(2,1)S(1)}, bf16[768,2048]{1,0:T(8,128)(2,1)}, u32[]{:S(2)}) copy-start(bf16[768,2048]{1,0:T(8,128)(2,1)} %param.26) | copy-start | bytes 9437188
  580.2 4.9 copy-start.3
  (30 other events, 17.7 us)
Sparse Core Ops, SparseCore 0:
  10.0 66.1 all-gather.4
  79.0 76.4 all-gather.2
